TPU v7x, 32 devices: a whole 2x2x4 slice. The times are simulated.
32 devices in a mesh: ep: 16 (over z, y, x), tp: 2 (over core).
Axes of the slice: x: 2, y: 2, z: 4, core: 2. Of those that a mesh axis runs over, the one named last changes fastest.
Arguments:
- tokens: bfloat16 [512, 3072], P('ep'), may hold values from -6 to 6
- carried: float32 [512, 96, 128], P('ep', 'tp'), may hold values from -4 to 4
- decay_rate: float32 [96, 64], P('tp'), may hold values from 0.02 to 20
- frequency: float32 [96, 64], P('tp'), may hold values from 0 to 200
- log_step: float32 [96], P('tp'), may hold values from -4.6 to 0
- in_map: bfloat16 [96, 128, 16], P('tp'), may hold values from -1 to 1
- out_map: bfloat16 [96, 16, 128], P('tp'), may hold values from -0.5 to 0.5
- skip_gain: float32 [1536], P('tp'), may hold values from -4 to 4
- norm_gain: float32 [3072], replicated, may hold values from 0.1 to 1.9
- w_in: bfloat16 [3072, 1536], P(None, 'tp'), may hold values from -0.109375 to 0.109375
- w_out: bfloat16 [1536, 3072], P('tp'), may hold values from -0.15625 to 0.15625
- expert_gain: float32 [3072], replicated, may hold values from 0.1 to 1.9
- route_ids: int32 [512, 2], P('ep'), may hold values from 0 to 7, all different within a row; in each aligned block of 32 rows (0 to 31, 32 to 63, ...) at most 16 rows name the same one
- route_logit: float32 [512, 2], P('ep'), may hold values from -6 to 6
- w_gate: bfloat16 [3072, 43008], P(None, ('ep', 'tp')), may hold values from -0.109375 to 0.109375
- w_up: bfloat16 [3072, 43008], P(None, ('ep', 'tp')), may hold values from -0.109375 to 0.109375
- w_down: bfloat16 [43008, 3072], P(('ep', 'tp')), may hold values from -0.078125 to 0.078125
Outputs:
- new_tokens: bfloat16 [512, 3072], P('ep', 'tp')
- new_carried: float32 [512, 96, 128], P('ep', 'tp')
Inputs may be any that keep to these rules, and one draw needn't show every extreme that they name: `route_ids`: each row names 2 different experts; within each aligned block of 32 rows (the rows of one index of ep) no expert is named by more than 16 rows, a bound that some block reaches.
All inputs are finite; a program needn't handle non-finite values.
Results may differ from a plain program's by a relative error of at most 0.014.
Values may be sent and summed in bfloat16 or wider, within the bound.
A program may use at most 128 MiB of HBM per device.

v0:
```python
import functools

import jax
import jax.numpy as jnp
from jax import lax
from jax.experimental import pallas as pl
from jax.experimental.pallas import tpu as pltpu
from jax.sharding import PartitionSpec as P

EXPERTS = 8
TOP = 2
CAP = 16


def normalize(rows, gain):
    wide = rows.astype(jnp.float32)
    scaled = wide * lax.rsqrt(jnp.mean(wide * wide, axis=-1, keepdims=True) + 1e-06)
    return (scaled * gain).astype(jnp.bfloat16)


def state_update(drive, carried, decay_rate, frequency, log_step, in_map, out_map, skip_gain):
    count_rows, width = drive.shape
    groups, half = decay_rate.shape
    channels = width // groups
    step_size = jnp.exp(log_step)[:, None]
    magnitude = jnp.exp(-decay_rate * step_size)
    real_decay = magnitude * jnp.cos(frequency * step_size)
    imag_decay = magnitude * jnp.sin(frequency * step_size)
    denom = decay_rate * decay_rate + frequency * frequency
    real_less = real_decay - 1.0
    real_factor = (-real_less * decay_rate + imag_decay * frequency) / denom
    imag_factor = (-imag_decay * decay_rate - real_less * frequency) / denom
    grouped_drive = drive.reshape(count_rows, groups, channels)
    projected = jnp.einsum(
        "sgh,gqh->sgq", grouped_drive, in_map, preferred_element_type=jnp.float32
    )
    real_in = projected[..., :half]
    imag_in = projected[..., half:]
    real_push = real_factor * real_in - imag_factor * imag_in
    imag_push = real_factor * imag_in + imag_factor * real_in
    real_old = carried[..., :half]
    imag_old = carried[..., half:]
    real_new = real_decay * real_old - imag_decay * imag_old + real_push
    imag_new = real_decay * imag_old + imag_decay * real_old + imag_push
    joined = jnp.concatenate([real_new, -imag_new], axis=-1)
    reading = jnp.einsum(
        "sgq,ghq->sgh", joined, out_map.astype(jnp.float32), precision=lax.Precision.HIGHEST
    )
    total = reading.reshape(count_rows, width) + skip_gain * drive.astype(jnp.float32)
    activated = jax.nn.gelu(total).astype(jnp.bfloat16)
    return (activated, jnp.concatenate([real_new, imag_new], axis=-1))


def route_weights(route_logit):
    first = jax.nn.sigmoid(route_logit[:, 0] - route_logit[:, 1])
    second = jax.nn.sigmoid(route_logit[:, 1] - route_logit[:, 0])
    return jnp.stack([first, second], axis=1)


MESH = pl.DeviceIdType.MESH
SEND_ORDER = (1, 2, 4, 6, 5, 7, 3)
WAIT_ORDER = (0, 1, 2, 4, 6, 5, 7, 3)
BACK_ORDER = (4, 6, 5, 7, 2, 3, 1)
PIECES = 3
BLOCK = 256


def dot_transposed(rows, weights):
    return lax.dot_general(
        rows, weights, (((1,), (1,)), ((), ())), preferred_element_type=jnp.float32
    )


def expert_kernel(
    group_size,
    tokens,
    activated,
    gain,
    pack,
    weight_high,
    weight_low,
    mix_hbm,
    gate_hbm,
    up_hbm,
    down_hbm,
    out,
    mix,
    gate,
    up,
    down,
    partial,
    partial_in,
    mixed_buf,
    normed_buf,
    packed,
    rows_buf,
    hidden,
    swap_out,
    swap_in,
    own_sum,
    peer_out,
    peer_in,
    back_out,
    returned,
    load_sem,
    partial_sem,
    direct_send,
    direct_recv,
    peer_send,
    peer_recv,
    core_send,
    core_recv,
    swap_send,
    swap_recv,
    sum_send,
    sum_recv,
    back_send,
    back_recv,
    local_sem,
):
    ep = lax.axis_index("ep")
    core = lax.axis_index("tp")
    expert = ep // group_size
    lane = ep % group_size
    other = 1 - core
    model_width = tokens.shape[1]
    half = model_width // 2
    hidden_units = gate_hbm.shape[0]
    sources = rows_buf.shape[1]
    total_rows = sources * CAP
    piece = half // PIECES

    def at_expert(step):
        place, bit = 0, 1
        while bit < EXPERTS:
            place = place + bit * lax.rem(expert // bit + step // bit, 2)
            bit *= 2
        return place

    def at_lane(step):
        return lax.rem(lane + step + group_size, group_size)

    mix_parts = 4
    mix_span = model_width // mix_parts
    mix_loads = []
    for part in range(mix_parts):
        span = pl.ds(part * mix_span, mix_span)
        mix_loads.append(
            pltpu.make_async_copy(mix_hbm.at[:, span], mix.at[:, span], load_sem.at[5 + part])
        )
        mix_loads[-1].start()
    loads = []
    for part in range(2):
        span = pl.ds(part * (hidden_units // 2), hidden_units // 2)
        loads.append(pltpu.make_async_copy(gate_hbm.at[span], gate.at[span], load_sem.at[2 * part]))
        loads.append(pltpu.make_async_copy(up_hbm.at[span], up.at[span], load_sem.at[2 * part + 1]))
    loads.append(pltpu.make_async_copy(down_hbm, down, load_sem.at[4]))

    barrier = pltpu.get_barrier_semaphore()
    pl.semaphore_signal(barrier, inc=1, device_id=(ep, other), device_id_type=MESH)
    for step in range(1, EXPERTS):
        target = at_expert(step) * group_size + lane
        pl.semaphore_signal(barrier, inc=1, device_id=(target, core), device_id_type=MESH)
    for step in range(1, group_size):
        target = expert * group_size + at_lane(step)
        pl.semaphore_signal(barrier, inc=1, device_id=(target, core), device_id_type=MESH)
    for part in range(mix_parts):
        span = pl.ds(part * mix_span, mix_span)
        mix_loads[part].wait()
        if part == mix_parts - 2:
            for load in loads:
                load.start()
        partial[:, span] = jnp.dot(
            activated[...], mix[:, span], preferred_element_type=jnp.float32
        ).astype(jnp.bfloat16)
    pl.semaphore_wait(barrier, EXPERTS + group_size - 1)

    def remote(source, target, send, recv, place):
        return pltpu.make_async_remote_copy(
            src_ref=source,
            dst_ref=target,
            send_sem=send,
            recv_sem=recv,
            device_id=place,
            device_id_type=MESH,
        )

    exchange = remote(partial, partial_in, partial_sem.at[0], partial_sem.at[1], (ep, other))
    exchange.start()
    exchange.wait()

    summed = partial[...].astype(jnp.float32) + partial_in[...].astype(jnp.float32)
    mixed = (tokens[...].astype(jnp.float32) + summed).astype(jnp.bfloat16)
    mixed_buf[...] = mixed
    normed_buf[...] = normalize(mixed, gain[...])
    own_columns = pl.ds(pl.multiple_of(core * half, 128), half)
    chosen = jnp.dot(pack[...], normed_buf[:, own_columns], preferred_element_type=jnp.float32)
    packed[...] = chosen.astype(jnp.bfloat16).reshape(EXPERTS, CAP, half)

    def direct(step):
        place = at_expert(step)
        return remote(
            packed.at[place],
            rows_buf.at[core, ep],
            direct_send.at[step],
            direct_recv.at[step],
            (place * group_size + lane, core),
        )

    def to_peer(step, shift):
        source = at_expert(step) * group_size + lane
        return remote(
            rows_buf.at[core, source],
            rows_buf.at[core, source],
            peer_send.at[shift, step],
            peer_recv.at[shift, step],
            (expert * group_size + at_lane(shift), core),
        )

    def to_core(step, shift):
        source = at_expert(step) * group_size + at_lane(-shift)
        return remote(
            rows_buf.at[core, source],
            rows_buf.at[core, source],
            core_send.at[shift, step],
            core_recv.at[shift, step],
            (ep, other),
        )

    def from_core(step, shift):
        source = at_expert(step) * group_size + at_lane(-shift)
        return remote(
            rows_buf.at[other, source],
            rows_buf.at[other, source],
            core_send.at[shift, step],
            core_recv.at[shift, step],
            (ep, other),
        )

    for step in SEND_ORDER:
        direct(step).start()
    own_copy = pltpu.make_async_copy(packed.at[expert], rows_buf.at[core, ep], local_sem)
    own_copy.start()
    for step in WAIT_ORDER:
        if step == 0:
            own_copy.wait()
        else:
            direct(step).wait_recv()
        for shift in range(1, group_size):
            to_peer(step, shift).start()
        to_core(step, 0).start()
    for step in WAIT_ORDER:
        for shift in range(1, group_size):
            to_peer(step, shift).wait_recv()
            to_core(step, shift).start()
    for step in WAIT_ORDER:
        for shift in range(group_size):
            from_core(step, shift).wait_recv()
    for load in loads[:4]:
        load.wait()

    def hidden_block(columns):
        low = rows_buf[0].reshape(total_rows, half)
        high = rows_buf[1].reshape(total_rows, half)

        def project(weights):
            return dot_transposed(low, weights[columns, :half]) + dot_transposed(
                high, weights[columns, half:]
            )

        hidden[:, columns] = (jax.nn.silu(project(gate)) * project(up)).astype(jnp.bfloat16)

    blocks = hidden_units // BLOCK

    def hidden_step(index, carry):
        hidden_block(pl.ds(pl.multiple_of(index * BLOCK, BLOCK), BLOCK))
        return carry

    lax.fori_loop(0, blocks, hidden_step, 0)
    if hidden_units % BLOCK:
        hidden_block(pl.ds(blocks * BLOCK, hidden_units % BLOCK))

    loads[4].wait()

    def produce(owner, index):
        columns = pl.ds(pl.multiple_of(owner * half + index * piece, 128), piece)
        return jnp.dot(hidden[...], down[:, columns], preferred_element_type=jnp.float32)

    def swap(index):
        return remote(
            swap_out.at[index],
            swap_in.at[index],
            swap_send.at[index],
            swap_recv.at[index],
            (ep, other),
        )

    def sum_to_peer(index, shift):
        place = at_lane(shift)
        return remote(
            peer_out.at[index, place],
            peer_in.at[index, shift - 1],
            sum_send.at[index, shift],
            sum_recv.at[index, shift],
            (expert * group_size + place, core),
        )

    def give_back(index, step):
        place = at_expert(step)
        return remote(
            back_out.at[index, place],
            returned.at[index, expert],
            back_send.at[index, step],
            back_recv.at[index, step],
            (place * group_size + lane, core),
        )

    def start_swap(index):
        swap_out[index] = produce(other, index).astype(jnp.bfloat16)
        swap(index).start()

    start_swap(0)
    for index in range(PIECES):
        if index + 1 < PIECES:
            start_swap(index + 1)
        value = produce(core, index)
        swap(index).wait_recv()
        value = value + swap_in[index].astype(jnp.float32)
        value = value.reshape(EXPERTS, group_size, CAP, piece)
        for place in range(group_size):
            own_sum[index, place] = value[:, place]
            peer_out[index, place] = value[:, place].astype(jnp.bfloat16)
        for shift in range(1, group_size):
            sum_to_peer(index, shift).start()
    for index in range(PIECES):
        value = own_sum[index, lane]
        for shift in range(1, group_size):
            sum_to_peer(index, shift).wait_recv()
            value = value + peer_in[index, shift - 1].astype(jnp.float32)
        back_out[index] = value.astype(jnp.bfloat16)
        for step in BACK_ORDER:
            give_back(index, step).start()
        returned[index, expert] = back_out[index, expert]
    for index in range(PIECES):
        for step in range(1, EXPERTS):
            give_back(index, step).wait_recv()
        rows = returned[index].reshape(EXPERTS * CAP, piece)
        value = jnp.dot(weight_high[...], rows, preferred_element_type=jnp.float32)
        value = value + jnp.dot(weight_low[...], rows, preferred_element_type=jnp.float32)
        columns = pl.ds(pl.multiple_of(core * half + index * piece, 128), piece)
        value = value + mixed_buf[:, columns].astype(jnp.float32)
        out[:, index * piece : (index + 1) * piece] = value.astype(out.dtype)

    for step in range(1, EXPERTS):
        direct(step).wait_send()
    for step in range(EXPERTS):
        for shift in range(group_size):
            to_core(step, shift).wait_send()
            if shift:
                to_peer(step, shift).wait_send()
    for index in range(PIECES):
        swap(index).wait_send()
        for shift in range(1, group_size):
            sum_to_peer(index, shift).wait_send()
        for step in range(1, EXPERTS):
            give_back(index, step).wait_send()


def experts(
    tokens, activated, gain, pack, weight_high, weight_low, w_out, w_gate, w_up, w_down
):
    count_rows, model_width = tokens.shape
    sources = lax.axis_size("ep")
    group_size = sources // EXPERTS
    half = model_width // 2
    piece = half // PIECES
    hidden_units = w_gate.shape[0]
    total_rows = sources * CAP
    peers = max(group_size - 1, 1)
    dma = pltpu.SemaphoreType.DMA
    narrow = jnp.bfloat16
    vmem = pl.BlockSpec(memory_space=pltpu.VMEM)
    anywhere = pl.BlockSpec(memory_space=pl.ANY)
    return pl.pallas_call(
        functools.partial(expert_kernel, group_size),
        out_shape=jax.ShapeDtypeStruct((count_rows, half), narrow),
        in_specs=[vmem] * 6 + [anywhere] * 4,
        out_specs=vmem,
        scratch_shapes=[
            pltpu.VMEM(w_out.shape, narrow),
            pltpu.VMEM(w_gate.shape, narrow),
            pltpu.VMEM(w_up.shape, narrow),
            pltpu.VMEM(w_down.shape, narrow),
            pltpu.VMEM((count_rows, model_width), narrow),
            pltpu.VMEM((count_rows, model_width), narrow),
            pltpu.VMEM((count_rows, model_width), narrow),
            pltpu.VMEM((count_rows, model_width), narrow),
            pltpu.VMEM((EXPERTS, CAP, half), narrow),
            pltpu.VMEM((2, sources, CAP, half), narrow),
            pltpu.VMEM((total_rows, hidden_units), narrow),
            pltpu.VMEM((PIECES, total_rows, piece), narrow),
            pltpu.VMEM((PIECES, total_rows, piece), narrow),
            pltpu.VMEM((PIECES, group_size, EXPERTS, CAP, piece), jnp.float32),
            pltpu.VMEM((PIECES, group_size, EXPERTS, CAP, piece), narrow),
            pltpu.VMEM((PIECES, peers, EXPERTS, CAP, piece), narrow),
            pltpu.VMEM((PIECES, EXPERTS, CAP, piece), narrow),
            pltpu.VMEM((PIECES, EXPERTS, CAP, piece), narrow),
            dma((9,)),
            dma((2,)),
            dma((EXPERTS,)),
            dma((EXPERTS,)),
            dma((group_size, EXPERTS)),
            dma((group_size, EXPERTS)),
            dma((group_size, EXPERTS)),
            dma((group_size, EXPERTS)),
            dma((PIECES,)),
            dma((PIECES,)),
            dma((PIECES, group_size)),
            dma((PIECES, group_size)),
            dma((PIECES, EXPERTS)),
            dma((PIECES, EXPERTS)),
            dma,
        ],
        compiler_params=pltpu.CompilerParams(
            collective_id=0, has_side_effects=True, vmem_limit_bytes=56 * 1024 * 1024
        ),
    )(tokens, activated, gain, pack, weight_high, weight_low, w_out, w_gate, w_up, w_down)


def per_device(
    tokens,
    carried,
    decay_rate,
    frequency,
    log_step,
    in_map,
    out_map,
    skip_gain,
    norm_gain,
    w_in,
    w_out,
    expert_gain,
    route_ids,
    route_logit,
    w_gate,
    w_up,
    w_down,
):
    count_rows, model_width = tokens.shape
    normed = normalize(tokens, norm_gain)
    drive = jnp.dot(normed, w_in, preferred_element_type=jnp.float32).astype(jnp.bfloat16)
    activated, new_carried = state_update(
        drive, carried, decay_rate, frequency, log_step, in_map, out_map, skip_gain
    )
    weights = route_weights(route_logit)
    expert_ids = jnp.arange(EXPERTS, dtype=jnp.int32)
    routes_flat = route_ids.reshape(-1)
    weights_flat = weights.reshape(-1)
    onehot = (routes_flat[:, None] == expert_ids[None, :]).astype(jnp.int32)
    earlier = jnp.cumsum(onehot, axis=0) - onehot
    slot_index = jnp.sum(earlier * onehot, axis=1)
    position = routes_flat * CAP + slot_index
    placement = (jnp.arange(EXPERTS * CAP, dtype=jnp.int32)[:, None] == position[None, :]).astype(
        jnp.float32
    )
    pack = placement.reshape(EXPERTS * CAP, count_rows, TOP).sum(axis=2).astype(jnp.bfloat16)
    weighing = (
        (placement * weights_flat[None, :]).reshape(EXPERTS * CAP, count_rows, TOP).sum(axis=2)
    ).T
    weight_high = lax.reduce_precision(weighing, 8, 7)
    weight_low = (weighing - weight_high).astype(jnp.bfloat16)
    weight_high = weight_high.astype(jnp.bfloat16)
    new_tokens = experts(
        tokens,
        activated,
        expert_gain.reshape(1, model_width),
        pack,
        weight_high,
        weight_low,
        w_out,
        w_gate.T,
        w_up.T,
        w_down,
    )
    return (new_tokens, new_carried)


def solution(mesh):
    return jax.shard_map(
        per_device,
        mesh=mesh,
        in_specs=(
            P("ep", None),
            P("ep", "tp", None),
            P("tp", None),
            P("tp", None),
            P("tp"),
            P("tp", None, None),
            P("tp", None, None),
            P("tp"),
            P(),
            P(None, "tp"),
            P("tp", None),
            P(),
            P("ep", None),
            P("ep", None),
            P(None, ("ep", "tp")),
            P(None, ("ep", "tp")),
            P(("ep", "tp"), None),
        ),
        out_specs=(P("ep", "tp"), P("ep", "tp", None)),
        check_vma=False,
    )
```

profile of v0, /device:TPU:0, one launch (start us, length us, event | category | flops | bytes accessed | tf_op | source)
XLA Modules:
  0.0 67.2 jit_solution(8011082789098410030)
XLA Ops:
  0.6 0.0 copy-start
  0.6 0.7 %exp.14 = f32[48]{0:T(128)S(1)} exponential(f32[48]{0:T(128)} %param.21) | non-fusion elementwise | bytes 384 | tf_op jit(solution)/shard_map/exp | solution.py:25
  1.3 0.9 %cosine_multiply_fusion = (f32[48,64]{1,0:T(8,128)S(1)}, f32[48,64]{1,0:T(8,128)S(1)}, f32[48,64]{1,0:T(8,128)S(1)}, f32[48,64]{1,0:T(8,128)S(1)}) fusion(f32[48,64]{1,0:T(8,128)} %param.20, f32[48,64]{1,0:T(8,128)} %param.19, f32[48]{0:T(128)S(1)} %exp.14), kind=kLoop, calls=%fused_computation.35 | loop fusion | flops 58368 | bytes 73920 | tf_op jit(solution)/shard_map/mul | solution.py:27
  2.3 1.6 %fusion.23 = (f32[32,48,64]{2,1,0:T(8,128)S(1)}, f32[32,48,64]{2,1,0:T(8,128)S(1)}) fusion(f32[32,48,128]{2,1,0:T(8,128)} %param.18), kind=kLoop, calls=%fused_computation.47 | loop fusion | bytes 1572864 | tf_op jit(solution)/shard_map/slice | solution.py:42
  3.9 1.1 %fusion.4 = f32[32]{0:T(128)S(1)} fusion(bf16[32,3072]{1,0:T(8,128)(2,1)} %tokens.1), kind=kLoop, calls=%fused_computation.11 | loop fusion | flops 294880 | bytes 196736 | tf_op jit(solution)/shard_map/reduce_sum | solution.py:17
  5.0 3.4 %convolution_convert_fusion = bf16[32,768]{1,0:T(8,128)(2,1)S(1)} fusion(bf16[3072,768]{1,0:T(8,128)(2,1)} %param.26, bf16[32,3072]{1,0:T(8,128)(2,1)} %tokens.1, f32[3072]{0:T(1024)} %param.25, f32[32]{0:T(128)S(1)} %add_rsqrt_fusion), kind=kOutput, calls=%fused_computation.1 | convolution fusion | flops 151412736 | bytes 4976768 | tf_op jit(solution)/shard_map/dot_general | solution.py:451
  8.5 0.2 copy.49
  8.6 0.0 copy-start.1
  8.6 0.0 copy-done
  8.6 0.0 copy-start.2
  8.7 0.0 copy-start.3
  8.7 0.0 copy-start.4
  8.7 0.3 convolution_bitcast_fusion
  9.0 0.8 %fusion.22 = (f32[32,48,64]{2,0,1:T(8,128)S(1)}, f32[32,48,64]{2,0,1:T(8,128)S(1)}, f32[32,48,64]{2,0,1:T(8,128)S(1)}) fusion(f32[32,48,128]{2,0,1:T(8,128)S(1)} %convolution_bitcast_fusion, f32[48,64]{1,0:T(8,128)S(1)} %get-tuple-element.19, f32[48,64]{1,0:T(8,128)S(1)} %get-tuple-element.20, f32[32,48,64]{2,1,0:T(8,128)S(1)} %get-tuple-element.16, ...), kind=kLoop, calls=%fused_computation.46 | loop fusion | flops 1474560 | bytes 2801664 | tf_op jit(solution)/shard_map/neg | solution.py:45
  9.8 0.0 copy-done.1
  9.8 0.8 %fusion = f32[48,32,16]{1,2,0:T(8,128)S(1)} fusion(bf16[48,16,128]{2,1,0:T(8,128)(2,1)S(1)} %copy-done.1, f32[32,48,64]{2,0,1:T(8,128)S(1)} %get-tuple-element.12, f32[32,48,64]{2,0,1:T(8,128)S(1)} %get-tuple-element.14), kind=kOutput, calls=%fused_computation.2 | convolution fusion | flops 37945344 | bytes 1081344 | tf_op jit(solution)/shard_map/sgq,ghq->sgh/dot_general | solution.py:46
  10.7 0.1 copy.50
  10.8 0.0 copy-done.2
  10.8 0.7 %fusion.17.activated = bf16[32,768]{1,0:T(8,128)(2,1)} fusion(f32[32,768]{1,0:T(8,128)S(1)} %copy.50, bf16[32,768]{1,0:T(8,128)(2,1)S(1)} %convolution_convert_fusion, f32[768]{0:T(1024)S(1)} %copy-done.2), kind=kLoop, calls=%fused_computation.24 | loop fusion | flops 294912 | bytes 199680 | tf_op jit(solution)/shard_map/convert_element_type | solution.py:50
  11.5 0.0 copy-done.3
  11.5 0.1 copy.51
  11.6 0.1 eq.31
  11.7 0.1 fusion.18
  11.7 0.1 reduce_window_sum.11
  11.8 0.2 select_reduce_fusion.1
  12.0 0.1 reduce_sum.40
  12.1 0.1 copy.52
  12.2 0.0 copy-done.4
  12.3 0.1 select_reduce_fusion
  12.4 0.6 fusion.20
  13.0 0.7 %copy.53.pack = bf16[128,32]{1,0:T(8,128)(2,1)} copy(bf16[128,32]{0,1:T(8,128)(2,1)S(1)} %get-tuple-element.11) | data formatting | bytes 16384 | tf_op jit(solution)/shard_map/convert_element_type | solution.py:466
  13.7 50.4 %shard_map.176 = bf16[32,1536]{1,0:T(8,128)(2,1)} custom-call(bf16[32,3072]{1,0:T(8,128)(2,1)} %tokens.1, bf16[32,768]{1,0:T(8,128)(2,1)} %fusion.17.activated, f32[1,3072]{1,0:T(1,128)} %bitcast.20, bf16[128,32]{1,0:T(8,128)(2,1)} %copy.53.pack, bf16[32,128]{1,0:T(8,128)(2,1)} %get-tuple-element.22.weight_high, ...), custom_call_target="tpu_custom_call" | custom-call | tf_op jit(solution)/shard_map/pallas_call | solution.py:384
  64.1 0.3 pad_maximum_fusion
  64.4 1.3 %copy.54 = f32[32,48,128]{2,1,0:T(8,128)} copy(f32[32,48,128]{2,0,1:T(8,128)S(1)} %pad_maximum_fusion) | data formatting | bytes 1572864
  65.7 1.5 %copy.64 = bf16[32,1536]{1,0:T(8,128)(2,1)} copy(bf16[32,1536]{1,0:T(8,128)(2,1)} %shard_map.176) | data formatting | bytes 196608
  (4 shorter events, 0.0 us)
Async XLA Ops:
  0.6 8.0 %copy-start = (bf16[48,128,16]{1,2,0:T(8,128)(2,1)S(1)}, bf16[48,128,16]{1,2,0:T(8,128)(2,1)}, u32[]{:S(2)}) copy-start(bf16[48,128,16]{1,2,0:T(8,128)(2,1)} %param.22) | copy-start | bytes 589828
  8.6 1.2 %copy-start.1 = (bf16[48,16,128]{2,1,0:T(8,128)(2,1)S(1)}, bf16[48,16,128]{2,1,0:T(8,128)(2,1)}, u32[]{:S(2)}) copy-start(bf16[48,16,128]{2,1,0:T(8,128)(2,1)} %param.23) | copy-start | bytes 589828
  8.6 2.1 %copy-start.2 = (f32[768]{0:T(1024)S(1)}, f32[768]{0:T(1024)}, u32[]{:S(2)}) copy-start(f32[768]{0:T(1024)} %param.24) | copy-start | bytes 9220
  8.7 2.8 %copy-start.3 = (s32[32,2]{0,1:T(2,128)S(1)}, s32[32,2]{0,1:T(2,128)}, u32[]{:S(2)}) copy-start(s32[32,2]{0,1:T(2,128)} %param.29) | copy-start | bytes 772
  8.7 3.6 %copy-start.4 = (f32[32,2]{0,1:T(2,128)S(1)}, f32[32,2]{0,1:T(2,128)}, u32[]{:S(2)}) copy-start(f32[32,2]{0,1:T(2,128)} %param.30) | copy-start | bytes 772
where the time goes:
time: 67.5 us; the launch traced here: 67.2 us
  Pallas kernels  50.4 us (75%)
  local copies, waits for them, and re-layouts  6.65 us (10%)
  other arithmetic  4.84 us (7%)
  matrix products  4.59 us (7%)
  between operations  0.77 us (1%)
    pallas_call x1, Pallas kernels, experts(): pl.pallas_call(functools.partial(expert_kernel, group_size), out_shape=ja...  50.4 us
    dot_general x1, matrix products, per_device(): jnp.dot(normed, w_in, preferred_element_type=jnp.float32)  3.43 us
    unnamed x13, local copies, waits for them, and re-layouts  3 us
    slice x1, local copies, waits for them, and re-layouts, state_update(): imag_old = carried[..., half:]  1.64 us

commit v1 on v0

v1 whole, which is shorter than its diff:
```python
import functools

import jax
import jax.numpy as jnp
from jax import lax
from jax.experimental import pallas as pl
from jax.experimental.pallas import tpu as pltpu
from jax.sharding import PartitionSpec as P

EXPERTS = 8
TOP = 2
CAP = 16

MESH = pl.DeviceIdType.MESH
SEND_ORDER = (1, 2, 4, 6, 5, 7, 3)
WAIT_ORDER = (0, 1, 2, 4, 6, 5, 7, 3)
BACK_ORDER = (4, 6, 5, 7, 2, 3, 1)
CHUNKS = 3
PIECES = 6
LANES = 128
OUT_PARTS = 4
WEIGHT_PARTS = 3


def normalize(rows, gain):
    wide = rows.astype(jnp.float32)
    scaled = wide * lax.rsqrt(jnp.mean(wide * wide, axis=-1, keepdims=True) + 1e-06)
    return (scaled * gain).astype(jnp.bfloat16)


def dot_wide(left, right):
    return jnp.dot(left, right, preferred_element_type=jnp.float32)


def dot_transposed(left, right):
    return lax.dot_general(
        left, right, (((1,), (1,)), ((), ())), preferred_element_type=jnp.float32
    )


def gelu(value):
    inner = 0.7978845608028654 * (value + 0.044715 * (value * value * value))
    return value * (0.5 * (1.0 + jnp.tanh(inner)))


def coefficients(log_step, decay_rate, frequency, tables):
    groups, half = decay_rate.shape
    row = lax.broadcasted_iota(jnp.int32, (groups, groups), 0)
    column = lax.broadcasted_iota(jnp.int32, (groups, groups), 1)
    spread = jnp.where(row == column, jnp.broadcast_to(log_step, (groups, groups)), 0.0)
    step_size = jnp.exp(jnp.sum(spread, axis=1, keepdims=True))
    magnitude = jnp.exp(-decay_rate * step_size)
    real_decay = magnitude * jnp.cos(frequency * step_size)
    imag_decay = magnitude * jnp.sin(frequency * step_size)
    denom = decay_rate * decay_rate + frequency * frequency
    real_less = real_decay - 1.0
    real_factor = (-real_less * decay_rate + imag_decay * frequency) / denom
    imag_factor = (-imag_decay * decay_rate - real_less * frequency) / denom
    tables[0] = jnp.concatenate([real_decay, real_decay], axis=1)
    tables[1] = jnp.concatenate([imag_decay, -imag_decay], axis=1)
    tables[2] = jnp.concatenate([real_factor, real_factor], axis=1)
    tables[3] = jnp.concatenate([imag_factor, -imag_factor], axis=1)


def routing(ids, logit):
    count_rows = ids.shape[1]
    expert = lax.broadcasted_iota(jnp.int32, (EXPERTS, count_rows), 0)
    first = (ids[0:1, :] == expert).astype(jnp.float32)
    second = (ids[1:2, :] == expert).astype(jnp.float32)
    named = first + second
    weight = first * jax.nn.sigmoid(logit[0:1, :] - logit[1:2, :])
    weight = weight + second * jax.nn.sigmoid(logit[1:2, :] - logit[0:1, :])
    row = lax.broadcasted_iota(jnp.int32, (count_rows, count_rows), 0)
    column = lax.broadcasted_iota(jnp.int32, (count_rows, count_rows), 1)
    earlier = dot_wide(named, (row < column).astype(jnp.float32))
    slots = (EXPERTS, CAP, count_rows)
    slot = lax.broadcasted_iota(jnp.int32, slots, 1).astype(jnp.float32)
    here = slot == jnp.broadcast_to(earlier[:, None, :], slots)
    pack = jnp.where(here, jnp.broadcast_to(named[:, None, :], slots), 0.0)
    weighed = jnp.where(here, jnp.broadcast_to(weight[:, None, :], slots), 0.0)
    total = EXPERTS * CAP
    return pack.reshape(total, count_rows), weighed.reshape(total, count_rows)


def layer_kernel(
    group_size,
    tokens_hbm,
    carried_hbm,
    decay_hbm,
    frequency_hbm,
    log_step_hbm,
    in_map_hbm,
    out_map_hbm,
    skip_hbm,
    norm_gain_hbm,
    w_in_hbm,
    w_out_hbm,
    expert_gain_hbm,
    ids_hbm,
    logit_hbm,
    gate_hbm,
    up_hbm,
    down_hbm,
    out,
    new_carried,
    tokens,
    carried,
    decay_rate,
    frequency,
    log_step,
    in_map,
    out_map,
    skip,
    norm_gain,
    expert_gain,
    ids,
    logit,
    gate_up,
    dense,
    tables,
    spread_in,
    spread_out,
    joined,
    activated,
    partial,
    partial_in,
    mixed_buf,
    normed_buf,
    packed,
    rows_buf,
    gate_sum,
    up_sum,
    hidden_t,
    hidden,
    swap_out,
    swap_in,
    own_sum,
    peer_out,
    peer_in,
    back_out,
    returned,
    load_sem,
    weight_sem,
    partial_send,
    partial_recv,
    direct_recv,
    peer_recv,
    core_recv,
    swap_recv,
    sum_recv,
    back_recv,
    send_sem,
):
    ep = lax.axis_index("ep")
    core = lax.axis_index("tp")
    expert = ep // group_size
    lane = ep % group_size
    other = 1 - core
    count_rows, model_width = tokens.shape
    groups, states = decay_rate.shape
    width = skip.shape[0]
    channels = width // groups
    per_block = LANES // channels
    blocks = groups // per_block
    half = model_width // 2
    hidden_units = gate_hbm.shape[0]
    total_rows = group_size * EXPERTS * CAP
    in_parts = model_width // width
    gate, up = gate_up.at[0], gate_up.at[1]
    mix = dense.at[width : 2 * width]
    down = dense.at[:hidden_units]
    piece = half // PIECES
    chunk = half // CHUNKS

    def at_expert(step):
        place, bit = 0, 1
        while bit < EXPERTS:
            place = place + bit * lax.rem(expert // bit + step // bit, 2)
            bit *= 2
        return place

    def at_lane(step):
        return lax.rem(lane + step + group_size, group_size)

    loads = {}

    def load(name, source, target):
        loads[name] = pltpu.make_async_copy(source, target, load_sem.at[len(loads)])
        loads[name].start()

    load("tokens", tokens_hbm, tokens)
    load("norm_gain", norm_gain_hbm, norm_gain)
    for part in range(in_parts):
        span = pl.ds(part * width, width)
        load(("w_in", part), w_in_hbm.at[span], dense.at[:width, span])
    load("log_step", log_step_hbm, log_step)
    load("decay", decay_hbm, decay_rate)
    load("frequency", frequency_hbm, frequency)
    load("in_map", in_map_hbm, in_map)
    load("out_map", out_map_hbm, out_map)
    load("carried", carried_hbm, carried)
    load("skip", skip_hbm, skip)
    load("ids", ids_hbm, ids)
    load("logit", logit_hbm, logit)
    load("expert_gain", expert_gain_hbm, expert_gain)
    out_span = model_width // OUT_PARTS
    for part in range(OUT_PARTS):
        span = pl.ds(part * out_span, out_span)
        load(("w_out", part), w_out_hbm.at[:, span], mix.at[:, span])

    barrier = pltpu.get_barrier_semaphore()
    pl.semaphore_signal(barrier, inc=1, device_id=(ep, other), device_id_type=MESH)
    for step in range(1, EXPERTS):
        target = at_expert(step) * group_size + lane
        pl.semaphore_signal(barrier, inc=1, device_id=(target, core), device_id_type=MESH)
    for step in range(1, group_size):
        target = expert * group_size + at_lane(step)
        pl.semaphore_signal(barrier, inc=1, device_id=(target, core), device_id_type=MESH)

    weight_span = hidden_units // WEIGHT_PARTS

    def weight_copies(source, target, sem):
        for part in range(WEIGHT_PARTS):
            span = pl.ds(part * weight_span, weight_span)
            pltpu.make_async_copy(source.at[span], target.at[span], sem).start()

    spread_in[...] = jnp.zeros_like(spread_in)
    spread_out[...] = jnp.zeros_like(spread_out)
    loads["tokens"].wait()
    loads["norm_gain"].wait()
    normed_buf[...] = normalize(tokens[...], norm_gain[...])
    for name in ("log_step", "decay", "frequency"):
        loads[name].wait()
    coefficients(log_step[...], decay_rate[...], frequency[...], tables)
    loads["in_map"].wait()
    loads["out_map"].wait()
    sign = jnp.where(lax.broadcasted_iota(jnp.int32, (1, LANES), 1) < states, 1.0, -1.0)
    for group in range(groups):
        block, place = divmod(group, per_block)
        rows = slice(place * channels, (place + 1) * channels)
        columns = slice(place * LANES, (place + 1) * LANES)
        tile = slice(group * channels, (group + 1) * channels)
        spread_in[block, rows, columns] = in_map[tile, :]
        spread_out[block, rows, columns] = (out_map[tile, :].astype(jnp.float32) * sign).astype(
            jnp.bfloat16
        )
    total = None
    for part in range(in_parts):
        loads["w_in", part].wait()
        span = slice(part * width, (part + 1) * width)
        term = dot_wide(normed_buf[:, span], dense[:width, span])
        total = term if total is None else total + term
    drive = total.astype(jnp.bfloat16)
    loads["carried"].wait()
    loads["skip"].wait()
    weight_copies(gate_hbm, gate, weight_sem.at[0])
    weight_copies(up_hbm, up, weight_sem.at[0])
    for block in range(blocks):
        lanes = slice(block * LANES, (block + 1) * LANES)
        projected = dot_wide(drive[:, lanes], spread_in[block])
        for place in range(per_block):
            group = block * per_block + place
            columns = slice(place * LANES, (place + 1) * LANES)
            entry = projected[:, columns]
            old = carried[pl.ds(group, count_rows, stride=groups), :]
            straight = tables[0, group : group + 1, :] * old
            straight = straight + tables[2, group : group + 1, :] * entry
            cross = tables[1, group : group + 1, :] * old
            cross = cross + tables[3, group : group + 1, :] * entry
            new = straight + pltpu.roll(cross, states, 1)
            new_carried[pl.ds(group, count_rows, stride=groups), :] = new
            high = new.astype(jnp.bfloat16)
            joined[block, :count_rows, columns] = high
            joined[block, count_rows:, columns] = (new - high.astype(jnp.float32)).astype(
                jnp.bfloat16
            )
        both = dot_transposed(joined[block], spread_out[block])
        read = both[:count_rows] + both[count_rows:]
        read = read + skip[lanes].reshape(1, LANES) * drive[:, lanes].astype(jnp.float32)
        activated[:, lanes] = gelu(read).astype(jnp.bfloat16)

    def remote(source, target, send, recv, place):
        return pltpu.make_async_remote_copy(
            src_ref=source,
            dst_ref=target,
            send_sem=send,
            recv_sem=recv,
            device_id=place,
            device_id_type=MESH,
        )

    def exchange(part):
        return remote(
            partial.at[part], partial_in.at[part], partial_send, partial_recv.at[part], (ep, other)
        )

    for part in range(OUT_PARTS):
        span = slice(part * out_span, (part + 1) * out_span)
        loads["w_out", part].wait()
        partial[part] = dot_wide(activated[...], mix[:, span]).astype(jnp.bfloat16)
        if part == 0:
            pl.semaphore_wait(barrier, EXPERTS + group_size - 1)
        exchange(part).start()
    weight_copies(down_hbm, down, weight_sem.at[1])

    loads["ids"].wait()
    loads["logit"].wait()
    loads["expert_gain"].wait()
    pack, weighed = routing(ids[...], logit[...])
    pack = pack.astype(jnp.bfloat16)
    weighed = weighed.T
    weight_high = weighed.astype(jnp.bfloat16)
    weight_low = (weighed - weight_high.astype(jnp.float32)).astype(jnp.bfloat16)

    for part in range(OUT_PARTS):
        span = slice(part * out_span, (part + 1) * out_span)
        exchange(part).wait_recv()
        summed = partial[part].astype(jnp.float32) + partial_in[part].astype(jnp.float32)
        mixed_buf[:, span] = (tokens[:, span].astype(jnp.float32) + summed).astype(jnp.bfloat16)
    normed_buf[...] = normalize(mixed_buf[...], expert_gain[...])

    def direct(index, step):
        place = at_expert(step)
        return remote(
            packed.at[index, place],
            rows_buf.at[index, core, lane, expert],
            send_sem.at[0],
            direct_recv.at[index, step],
            (place * group_size + lane, core),
        )

    def to_peer(index, step, shift):
        source = at_expert(step)
        return remote(
            rows_buf.at[index, core, lane, source],
            rows_buf.at[index, core, lane, source],
            send_sem.at[1],
            peer_recv.at[index, shift],
            (expert * group_size + at_lane(shift), core),
        )

    def from_peer(index, shift):
        block = rows_buf.at[index, core, at_lane(-shift)]
        place = (expert * group_size + at_lane(shift), core)
        return remote(block, block, send_sem.at[1], peer_recv.at[index, shift], place)

    def across(index, shift):
        block = rows_buf.at[index, core, at_lane(-shift)]
        return remote(block, block, send_sem.at[2], core_recv.at[index], (ep, other))

    def from_core(index):
        block = rows_buf.at[index, other]
        return remote(block, block, send_sem.at[2], core_recv.at[index], (ep, other))

    for index in range(CHUNKS):
        columns = pl.ds(pl.multiple_of(core * half + index * chunk, LANES), chunk)
        chosen = dot_wide(pack, normed_buf[:, columns]).astype(jnp.bfloat16)
        packed[index] = chosen.reshape(EXPERTS, CAP, chunk)
        for step in SEND_ORDER:
            direct(index, step).start()
        rows_buf[index, core, lane, expert] = packed[index, expert]

    def relay(index):
        for step in WAIT_ORDER:
            if step:
                direct(index, step).wait_recv()
            for shift in range(1, group_size):
                to_peer(index, step, shift).start()
        across(index, 0).start()

    def cross(index):
        for shift in range(1, group_size):
            from_peer(index, shift).wait_recv()
            across(index, shift).start()

    height = hidden_units if hidden_units < 1024 else hidden_units // 2

    def accumulate(index):
        low = slice(index * chunk, (index + 1) * chunk)
        high = slice(half + index * chunk, half + (index + 1) * chunk)

        def part(number, carry):
            units = pl.ds(pl.multiple_of(number * height, 16), height)

            def project(weights):
                value = dot_transposed(
                    weights[units, low], rows_buf[index, 0].reshape(total_rows, chunk)
                )
                return value + dot_transposed(
                    weights[units, high], rows_buf[index, 1].reshape(total_rows, chunk)
                )

            gated = project(gate)
            upward = project(up)
            if index:
                gated = gate_sum[units, :] + gated
                upward = up_sum[units, :] + upward
            if index < CHUNKS - 1:
                gate_sum[units, :] = gated
                up_sum[units, :] = upward
            else:
                hidden_t[units, :] = (jax.nn.silu(gated) * upward).astype(jnp.bfloat16)
            return carry

        lax.fori_loop(0, hidden_units // height, part, 0)

    relay(0)
    for index in range(CHUNKS):
        if index + 1 < CHUNKS:
            relay(index + 1)
        cross(index)
        from_core(index).wait_recv()
        if index == 0:
            pltpu.make_async_copy(gate_up, gate_up, weight_sem.at[0]).wait()
        accumulate(index)
    for start in range(0, hidden_units, LANES):
        units = slice(start, min(start + LANES, hidden_units))
        hidden[:, units] = hidden_t[units, :].T
    pltpu.make_async_copy(down, down, weight_sem.at[1]).wait()

    def produce(owner, index):
        columns = pl.ds(pl.multiple_of(owner * half + index * piece, 128), piece)
        return jnp.dot(hidden[...], down[:, columns], preferred_element_type=jnp.float32)

    def swap(index):
        return remote(
            swap_out.at[index], swap_in.at[index], send_sem.at[3], swap_recv.at[index], (ep, other)
        )

    def sum_to_peer(index, shift):
        place = at_lane(shift)
        return remote(
            peer_out.at[index, place],
            peer_in.at[index, shift - 1],
            send_sem.at[4],
            sum_recv.at[index],
            (expert * group_size + place, core),
        )

    def from_peers(index):
        block = peer_in.at[index]
        return remote(block, block, send_sem.at[4], sum_recv.at[index], (ep, other))

    def give_back(index, step):
        place = at_expert(step)
        return remote(
            back_out.at[index, place],
            returned.at[index, expert],
            send_sem.at[5],
            back_recv.at[index],
            (place * group_size + lane, core),
        )

    def given_back(index):
        block = returned.at[index, : EXPERTS - 1]
        return remote(block, block, send_sem.at[5], back_recv.at[index], (ep, other))

    def start_swap(index):
        swap_out[index] = produce(other, index).astype(jnp.bfloat16)
        swap(index).start()

    start_swap(0)
    for index in range(PIECES):
        if index + 1 < PIECES:
            start_swap(index + 1)
        value = produce(core, index)
        swap(index).wait_recv()
        value = value + swap_in[index].astype(jnp.float32)
        value = value.reshape(group_size, EXPERTS, CAP, piece)
        own_sum[index] = value
        peer_out[index] = value.astype(jnp.bfloat16)
        for shift in range(1, group_size):
            sum_to_peer(index, shift).start()
    for index in range(PIECES):
        value = own_sum[index, lane]
        if group_size > 1:
            from_peers(index).wait_recv()
        for shift in range(1, group_size):
            value = value + peer_in[index, shift - 1].astype(jnp.float32)
        back_out[index] = value.astype(jnp.bfloat16)
        for step in BACK_ORDER:
            give_back(index, step).start()
        returned[index, expert] = back_out[index, expert]
    for index in range(PIECES):
        given_back(index).wait_recv()
        rows = returned[index].reshape(EXPERTS * CAP, piece)
        value = jnp.dot(weight_high, rows, preferred_element_type=jnp.float32)
        value = value + jnp.dot(weight_low, rows, preferred_element_type=jnp.float32)
        columns = pl.ds(pl.multiple_of(core * half + index * piece, 128), piece)
        value = value + mixed_buf[:, columns].astype(jnp.float32)
        out[:, index * piece : (index + 1) * piece] = value.astype(out.dtype)


    def sent(block, sem):
        remote(block, block, sem, sem, (ep, other)).wait_send()

    sent(partial, partial_send)
    sent(packed.at[:, : EXPERTS - 1], send_sem.at[0])
    if group_size > 1:
        sent(rows_buf.at[:, core, : group_size - 1], send_sem.at[1])
        sent(peer_out.at[:, : group_size - 1], send_sem.at[4])
    sent(rows_buf.at[:, core], send_sem.at[2])
    sent(swap_out, send_sem.at[3])
    sent(back_out.at[:, : EXPERTS - 1], send_sem.at[5])


def per_device(
    tokens,
    carried,
    decay_rate,
    frequency,
    log_step,
    in_map,
    out_map,
    skip_gain,
    norm_gain,
    w_in,
    w_out,
    expert_gain,
    route_ids,
    route_logit,
    w_gate,
    w_up,
    w_down,
):
    count_rows, model_width = tokens.shape
    groups, states = decay_rate.shape
    width = skip_gain.shape[0]
    per_block = LANES * groups // width
    blocks = groups // per_block
    sources = lax.axis_size("ep")
    group_size = sources // EXPERTS
    half = model_width // 2
    piece = half // PIECES
    chunk = half // CHUNKS
    hidden_units = w_down.shape[0]
    total_rows = sources * CAP
    peers = max(group_size - 1, 1)
    dma = pltpu.SemaphoreType.DMA
    narrow = jnp.bfloat16
    wide = jnp.float32
    vmem = pl.BlockSpec(memory_space=pltpu.VMEM)
    far = pl.BlockSpec(memory_space=pltpu.HBM)
    operands = (
        tokens,
        carried.reshape(count_rows * groups, 2 * states),
        decay_rate,
        frequency,
        log_step.reshape(1, groups),
        in_map.transpose(0, 2, 1).reshape(width, 2 * states),
        out_map.reshape(width, 2 * states),
        skip_gain,
        norm_gain.reshape(1, model_width),
        w_in,
        w_out,
        expert_gain.reshape(1, model_width),
        route_ids.T,
        route_logit.T,
        w_gate.T,
        w_up.T,
        w_down,
    )
    staged = operands[:9] + operands[11:14]
    new_tokens, new_carried = pl.pallas_call(
        functools.partial(layer_kernel, group_size),
        out_shape=(
            jax.ShapeDtypeStruct((count_rows, half), narrow),
            jax.ShapeDtypeStruct((count_rows * groups, 2 * states), wide),
        ),
        in_specs=[far] * len(operands),
        out_specs=(vmem, vmem),
        scratch_shapes=[pltpu.VMEM(value.shape, value.dtype) for value in staged]
        + [
            pltpu.VMEM((2, hidden_units, model_width), narrow),
            pltpu.VMEM((max(2 * width, hidden_units), model_width), narrow),
            pltpu.VMEM((4, groups, 2 * states), wide),
            pltpu.VMEM((blocks, LANES, per_block * LANES), narrow),
            pltpu.VMEM((blocks, LANES, per_block * LANES), narrow),
            pltpu.VMEM((blocks, 2 * count_rows, per_block * LANES), narrow),
            pltpu.VMEM((count_rows, width), narrow),
            pltpu.VMEM((OUT_PARTS, count_rows, model_width // OUT_PARTS), narrow),
            pltpu.VMEM((OUT_PARTS, count_rows, model_width // OUT_PARTS), narrow),
            pltpu.VMEM((count_rows, model_width), narrow),
            pltpu.VMEM((count_rows, model_width), narrow),
            pltpu.VMEM((CHUNKS, EXPERTS, CAP, chunk), narrow),
            pltpu.VMEM((CHUNKS, 2, group_size, EXPERTS, CAP, chunk), narrow),
            pltpu.VMEM((hidden_units, total_rows), wide),
            pltpu.VMEM((hidden_units, total_rows), wide),
            pltpu.VMEM((hidden_units, total_rows), narrow),
            pltpu.VMEM((total_rows, hidden_units), narrow),
            pltpu.VMEM((PIECES, total_rows, piece), narrow),
            pltpu.VMEM((PIECES, total_rows, piece), narrow),
            pltpu.VMEM((PIECES, group_size, EXPERTS, CAP, piece), wide),
            pltpu.VMEM((PIECES, group_size, EXPERTS, CAP, piece), narrow),
            pltpu.VMEM((PIECES, peers, EXPERTS, CAP, piece), narrow),
            pltpu.VMEM((PIECES, EXPERTS, CAP, piece), narrow),
            pltpu.VMEM((PIECES, EXPERTS, CAP, piece), narrow),
            dma((len(staged) + model_width // width + OUT_PARTS,)),
            dma((2,)),
            dma,
            dma((OUT_PARTS,)),
            dma((CHUNKS, EXPERTS)),
            dma((CHUNKS, group_size)),
            dma((CHUNKS,)),
            dma((PIECES,)),
            dma((PIECES,)),
            dma((PIECES,)),
            dma((6,)),
        ],
        compiler_params=pltpu.CompilerParams(
            collective_id=0, has_side_effects=True, vmem_limit_bytes=50 * 1024 * 1024
        ),
    )(*[pltpu.with_memory_space_constraint(value, pltpu.HBM) for value in operands])
    return (new_tokens, new_carried.reshape(count_rows, groups, 2 * states))


def solution(mesh):
    return jax.shard_map(
        per_device,
        mesh=mesh,
        in_specs=(
            P("ep", None),
            P("ep", "tp", None),
            P("tp", None),
            P("tp", None),
            P("tp"),
            P("tp", None, None),
            P("tp", None, None),
            P("tp"),
            P(),
            P(None, "tp"),
            P("tp", None),
            P(),
            P("ep", None),
            P("ep", None),
            P(None, ("ep", "tp")),
            P(None, ("ep", "tp")),
            P(("ep", "tp"), None),
        ),
        out_specs=(P("ep", "tp"), P("ep", "tp", None)),
        check_vma=False,
    )
```

time: 67.5 us -> 54.5 us (0.81)
  local copies, waits for them, and re-layouts: 6.65 us -> 1.52 us
  other arithmetic: 4.84 us -> 0 us
  matrix products: 4.59 us -> 0 us
  Pallas kernels: 50.4 us -> 52.2 us
    dot_general x3 -> x0, matrix products: 4.59 us -> none  [the longest x1 3.43 us: per_device(): jnp.dot(normed, w_in, preferred_element_type=jnp.float32)]
    pallas_call x1, Pallas kernels: 50.4 us -> 52.2 us  [per_device(): pl.pallas_call(functools.partial(layer_kernel, group_size), out_shape=(ja...]
    slice x1 -> x0, local copies, waits for them, and re-layouts: 1.64 us -> none  [state_update(): imag_old = carried[..., half:]]
    unnamed x13 -> x2, local copies, waits for them, and re-layouts: 3 us -> 1.52 us
    convert_element_type x3 -> x0, other arithmetic: 1.36 us -> none  [the longest x1 0.68 us: state_update(): activated = jax.nn.gelu(total).astype(jnp.bfloat16)]
    reduce_sum x3 -> x0, other arithmetic: 1.34 us -> none  [the longest x1 1.08 us: normalize(): jnp.mean(wide * wide, axis=-1, keepdims=True) + 1e-06]
    mul x1 -> x0, other arithmetic: 0.94 us -> none  [state_update(): real_decay = magnitude * jnp.cos(frequency * step_size)]
    convert_element_type x2 -> x0, local copies, waits for them, and re-layouts: 0.89 us -> none  [the longest x1 0.72 us: per_device(): placement.reshape(EXPERTS * CAP, count_rows, TOP).sum(axis=2)]
where the time goes in v1:
time: 54.5 us; the launch traced here: 54.4 us
  Pallas kernels  52.2 us (96%)
  local copies, waits for them, and re-layouts  1.52 us (3%)
  between operations  0.65 us (1%)
    pallas_call x1, Pallas kernels, per_device(): pl.pallas_call(functools.partial(layer_kernel, group_size), out_shape=(ja...  52.2 us
    unnamed x2, local copies, waits for them, and re-layouts  1.52 us

profile of v1, /device:TPU:0, one launch (start us, length us, event | category | flops | bytes accessed | tf_op | source)
XLA Modules:
  0.0 54.4 jit_solution(9652825409866580837)
XLA Ops:
  0.6 52.2 %shard_map.176 = (bf16[32,1536]{1,0:T(8,128)(2,1)S(1)}, f32[1536,128]{1,0:T(8,128)S(1)}) custom-call(bf16[32,3072]{1,0:T(8,128)(2,1)} %tokens_hbm.1, f32[1536,128]{1,0:T(8,128)} %bitcast.16, f32[48,64]{1,0:T(8,128)} %decay_hbm.1, f32[48,64]{1,0:T(8,128)} %frequency_hbm.1, f32[1,48]{1,0:T(1,128)} %bitcast.23, bf16[768,128]{1,0:T(8,128)(2,1)} %bitcast.17, ...), custom_call_target="tpu_custom_call" | custom-call | tf_op jit(solution)/shard_map/pallas_call | solution.py:564
  52.9 0.6 %copy.21 = bf16[32,1536]{1,0:T(8,128)(2,1)} copy(bf16[32,1536]{1,0:T(8,128)(2,1)S(1)} %get-tuple-element.8) | data formatting | bytes 196608
  53.5 0.9 %copy.22 = f32[32,48,128]{2,1,0:T(8,128)} copy(f32[32,48,128]{2,1,0:T(8,128)S(1)} %bitcast.13) | data formatting | bytes 1572864

commit v2 on v1

--- a/solution.py
+++ b/solution.py
@@ -12,14 +12,23 @@
 CAP = 16
 
 MESH = pl.DeviceIdType.MESH
-SEND_ORDER = (1, 2, 4, 6, 5, 7, 3)
-WAIT_ORDER = (0, 1, 2, 4, 6, 5, 7, 3)
+SEND_ORDER = (1, 3, 2, 5, 4, 7, 6)
+WAIT_ORDER = (0, 1, 2, 3, 4, 5, 6, 7)
 BACK_ORDER = (4, 6, 5, 7, 2, 3, 1)
-CHUNKS = 3
-PIECES = 6
+CHUNK_SHARES = (3, 3)
+PIECE_SHARES = (2, 2, 2)
+STRIP = 256
+UNIT_PARTS = 2
 LANES = 128
+LATE_PART = 1
 OUT_PARTS = 4
 WEIGHT_PARTS = 3
+
+
+def parts_of(length, shares):
+    unit = length // sum(shares)
+    starts = [unit * sum(shares[:index]) for index in range(len(shares))]
+    return [(start, unit * share) for start, share in zip(starts, shares)]
 
 
 def normalize(rows, gain):
@@ -143,13 +152,18 @@
     weight_sem,
     partial_send,
     partial_recv,
+    direct_send,
     direct_recv,
+    peer_send,
     peer_recv,
+    core_send,
     core_recv,
+    swap_send,
     swap_recv,
+    sum_send,
     sum_recv,
+    back_send,
     back_recv,
-    send_sem,
 ):
     ep = lax.axis_index("ep")
     core = lax.axis_index("tp")
@@ -169,8 +183,9 @@
     gate, up = gate_up.at[0], gate_up.at[1]
     mix = dense.at[width : 2 * width]
     down = dense.at[:hidden_units]
-    piece = half // PIECES
-    chunk = half // CHUNKS
+    pieces = parts_of(half, PIECE_SHARES)
+    strips = half // STRIP
+    chunks = parts_of(half, CHUNK_SHARES)
 
     def at_expert(step):
         place, bit = 0, 1
@@ -204,9 +219,6 @@
     load("logit", logit_hbm, logit)
     load("expert_gain", expert_gain_hbm, expert_gain)
     out_span = model_width // OUT_PARTS
-    for part in range(OUT_PARTS):
-        span = pl.ds(part * out_span, out_span)
-        load(("w_out", part), w_out_hbm.at[:, span], mix.at[:, span])
 
     barrier = pltpu.get_barrier_semaphore()
     pl.semaphore_signal(barrier, inc=1, device_id=(ep, other), device_id_type=MESH)
@@ -247,6 +259,10 @@
     total = None
     for part in range(in_parts):
         loads["w_in", part].wait()
+        if part == LATE_PART:
+            for late in range(OUT_PARTS):
+                span = pl.ds(late * out_span, out_span)
+                load(("w_out", late), w_out_hbm.at[:, span], mix.at[:, span])
         span = slice(part * width, (part + 1) * width)
         term = dot_wide(normed_buf[:, span], dense[:width, span])
         total = term if total is None else total + term
@@ -322,43 +338,38 @@
     def direct(index, step):
         place = at_expert(step)
         return remote(
-            packed.at[index, place],
-            rows_buf.at[index, core, lane, expert],
-            send_sem.at[0],
+            packed[index].at[place],
+            rows_buf[index].at[core, lane, expert],
+            direct_send.at[index],
             direct_recv.at[index, step],
             (place * group_size + lane, core),
         )
 
     def to_peer(index, step, shift):
-        source = at_expert(step)
-        return remote(
-            rows_buf.at[index, core, lane, source],
-            rows_buf.at[index, core, lane, source],
-            send_sem.at[1],
-            peer_recv.at[index, shift],
-            (expert * group_size + at_lane(shift), core),
-        )
+        block = rows_buf[index].at[core, lane, at_expert(step)]
+        place = (expert * group_size + at_lane(shift), core)
+        return remote(block, block, peer_send.at[index], peer_recv.at[index, shift], place)
 
     def from_peer(index, shift):
-        block = rows_buf.at[index, core, at_lane(-shift)]
+        block = rows_buf[index].at[core, at_lane(-shift)]
         place = (expert * group_size + at_lane(shift), core)
-        return remote(block, block, send_sem.at[1], peer_recv.at[index, shift], place)
+        return remote(block, block, peer_send.at[index], peer_recv.at[index, shift], place)
 
     def across(index, shift):
-        block = rows_buf.at[index, core, at_lane(-shift)]
-        return remote(block, block, send_sem.at[2], core_recv.at[index], (ep, other))
+        block = rows_buf[index].at[core, at_lane(-shift)]
+        return remote(block, block, core_send.at[index], core_recv.at[index], (ep, other))
 
     def from_core(index):
-        block = rows_buf.at[index, other]
-        return remote(block, block, send_sem.at[2], core_recv.at[index], (ep, other))
-
-    for index in range(CHUNKS):
-        columns = pl.ds(pl.multiple_of(core * half + index * chunk, LANES), chunk)
+        block = rows_buf[index].at[other]
+        return remote(block, block, core_send.at[index], core_recv.at[index], (ep, other))
+
+    for index, (begin, size) in enumerate(chunks):
+        columns = pl.ds(pl.multiple_of(core * half + begin, LANES), size)
         chosen = dot_wide(pack, normed_buf[:, columns]).astype(jnp.bfloat16)
-        packed[index] = chosen.reshape(EXPERTS, CAP, chunk)
+        packed[index][...] = chosen.reshape(EXPERTS, CAP, size)
         for step in SEND_ORDER:
             direct(index, step).start()
-        rows_buf[index, core, lane, expert] = packed[index, expert]
+        rows_buf[index][core, lane, expert] = packed[index][expert]
 
     def relay(index):
         for step in WAIT_ORDER:
@@ -373,58 +384,61 @@
             from_peer(index, shift).wait_recv()
             across(index, shift).start()
 
-    height = hidden_units if hidden_units < 1024 else hidden_units // 2
-
-    def accumulate(index):
-        low = slice(index * chunk, (index + 1) * chunk)
-        high = slice(half + index * chunk, half + (index + 1) * chunk)
-
-        def part(number, carry):
-            units = pl.ds(pl.multiple_of(number * height, 16), height)
-
-            def project(weights):
-                value = dot_transposed(
-                    weights[units, low], rows_buf[index, 0].reshape(total_rows, chunk)
-                )
-                return value + dot_transposed(
-                    weights[units, high], rows_buf[index, 1].reshape(total_rows, chunk)
-                )
-
-            gated = project(gate)
-            upward = project(up)
-            if index:
-                gated = gate_sum[units, :] + gated
-                upward = up_sum[units, :] + upward
-            if index < CHUNKS - 1:
-                gate_sum[units, :] = gated
-                up_sum[units, :] = upward
-            else:
-                hidden_t[units, :] = (jax.nn.silu(gated) * upward).astype(jnp.bfloat16)
-            return carry
-
-        lax.fori_loop(0, hidden_units // height, part, 0)
+    height = hidden_units // UNIT_PARTS
+
+    def accumulate(index, number):
+        begin, size = chunks[index]
+        units = slice(number * height, (number + 1) * height)
+        arrived = rows_buf[index]
+
+        def project(weights):
+            value = dot_transposed(
+                weights[units, begin : begin + size], arrived[0].reshape(total_rows, size)
+            )
+            return value + dot_transposed(
+                weights[units, half + begin : half + begin + size],
+                arrived[1].reshape(total_rows, size),
+            )
+
+        gated = project(gate)
+        upward = project(up)
+        if index:
+            gated = gate_sum[units, :] + gated
+            upward = up_sum[units, :] + upward
+        if index < len(chunks) - 1:
+            gate_sum[units, :] = gated
+            up_sum[units, :] = upward
+        else:
+            hidden_t[units, :] = (jax.nn.silu(gated) * upward).astype(jnp.bfloat16)
+
+    def transpose(begin, end):
+        for start in range(begin, end, LANES):
+            units = slice(start, min(start + LANES, end))
+            hidden[:, units] = hidden_t[units, :].T
 
     relay(0)
-    for index in range(CHUNKS):
-        if index + 1 < CHUNKS:
+    for index in range(len(chunks)):
+        if index + 1 < len(chunks):
             relay(index + 1)
-        cross(index)
+        if index == 0:
+            cross(0)
+            pltpu.make_async_copy(gate_up, gate_up, weight_sem.at[0]).wait()
         from_core(index).wait_recv()
-        if index == 0:
-            pltpu.make_async_copy(gate_up, gate_up, weight_sem.at[0]).wait()
-        accumulate(index)
-    for start in range(0, hidden_units, LANES):
-        units = slice(start, min(start + LANES, hidden_units))
-        hidden[:, units] = hidden_t[units, :].T
+        for number in range(UNIT_PARTS):
+            accumulate(index, number)
+            if number == 0 and index + 1 < len(chunks):
+                cross(index + 1)
+    transpose(0, hidden_units)
     pltpu.make_async_copy(down, down, weight_sem.at[1]).wait()
 
     def produce(owner, index):
-        columns = pl.ds(pl.multiple_of(owner * half + index * piece, 128), piece)
+        begin, size = pieces[index]
+        columns = pl.ds(pl.multiple_of(owner * half + begin, LANES), size)
         return jnp.dot(hidden[...], down[:, columns], preferred_element_type=jnp.float32)
 
     def swap(index):
         return remote(
-            swap_out.at[index], swap_in.at[index], send_sem.at[3], swap_recv.at[index], (ep, other)
+            swap_out[index], swap_in[index], swap_send.at[index], swap_recv.at[index], (ep, other)
         )
 
     def sum_to_peer(index, shift):
@@ -432,46 +446,49 @@
         return remote(
             peer_out.at[index, place],
             peer_in.at[index, shift - 1],
-            send_sem.at[4],
+            sum_send,
             sum_recv.at[index],
             (expert * group_size + place, core),
         )
 
     def from_peers(index):
         block = peer_in.at[index]
-        return remote(block, block, send_sem.at[4], sum_recv.at[index], (ep, other))
+        return remote(block, block, sum_send, sum_recv.at[index], (ep, other))
 
     def give_back(index, step):
         place = at_expert(step)
         return remote(
             back_out.at[index, place],
             returned.at[index, expert],
-            send_sem.at[5],
+            back_send,
             back_recv.at[index],
             (place * group_size + lane, core),
         )
 
     def given_back(index):
         block = returned.at[index, : EXPERTS - 1]
-        return remote(block, block, send_sem.at[5], back_recv.at[index], (ep, other))
+        return remote(block, block, back_send, back_recv.at[index], (ep, other))
 
     def start_swap(index):
-        swap_out[index] = produce(other, index).astype(jnp.bfloat16)
+        swap_out[index][...] = produce(other, index).astype(jnp.bfloat16)
         swap(index).start()
 
     start_swap(0)
-    for index in range(PIECES):
-        if index + 1 < PIECES:
+    for index, (begin, size) in enumerate(pieces):
+        if index + 1 < len(pieces):
             start_swap(index + 1)
         value = produce(core, index)
         swap(index).wait_recv()
-        value = value + swap_in[index].astype(jnp.float32)
-        value = value.reshape(group_size, EXPERTS, CAP, piece)
-        own_sum[index] = value
-        peer_out[index] = value.astype(jnp.bfloat16)
-        for shift in range(1, group_size):
-            sum_to_peer(index, shift).start()
-    for index in range(PIECES):
+        value = value + swap_in[index][...].astype(jnp.float32)
+        for inner in range(0, size, STRIP):
+            strip = (begin + inner) // STRIP
+            shape = (group_size, EXPERTS, CAP, STRIP)
+            columns = value[:, inner : inner + STRIP].reshape(shape)
+            own_sum[strip] = columns
+            peer_out[strip] = columns.astype(jnp.bfloat16)
+            for shift in range(1, group_size):
+                sum_to_peer(strip, shift).start()
+    for index in range(strips):
         value = own_sum[index, lane]
         if group_size > 1:
             from_peers(index).wait_recv()
@@ -481,27 +498,29 @@
         for step in BACK_ORDER:
             give_back(index, step).start()
         returned[index, expert] = back_out[index, expert]
-    for index in range(PIECES):
+    for index in range(strips):
         given_back(index).wait_recv()
-        rows = returned[index].reshape(EXPERTS * CAP, piece)
+        rows = returned[index].reshape(EXPERTS * CAP, STRIP)
         value = jnp.dot(weight_high, rows, preferred_element_type=jnp.float32)
         value = value + jnp.dot(weight_low, rows, preferred_element_type=jnp.float32)
-        columns = pl.ds(pl.multiple_of(core * half + index * piece, 128), piece)
+        columns = pl.ds(pl.multiple_of(core * half + index * STRIP, LANES), STRIP)
         value = value + mixed_buf[:, columns].astype(jnp.float32)
-        out[:, index * piece : (index + 1) * piece] = value.astype(out.dtype)
-
+        out[:, index * STRIP : (index + 1) * STRIP] = value.astype(out.dtype)
 
     def sent(block, sem):
         remote(block, block, sem, sem, (ep, other)).wait_send()
 
     sent(partial, partial_send)
-    sent(packed.at[:, : EXPERTS - 1], send_sem.at[0])
+    for index in range(len(chunks)):
+        sent(packed[index].at[: EXPERTS - 1], direct_send.at[index])
+        if group_size > 1:
+            sent(rows_buf[index].at[core, : group_size - 1], peer_send.at[index])
+        sent(rows_buf[index].at[core], core_send.at[index])
+    for index in range(len(pieces)):
+        sent(swap_out[index], swap_send.at[index])
     if group_size > 1:
-        sent(rows_buf.at[:, core, : group_size - 1], send_sem.at[1])
-        sent(peer_out.at[:, : group_size - 1], send_sem.at[4])
-    sent(rows_buf.at[:, core], send_sem.at[2])
-    sent(swap_out, send_sem.at[3])
-    sent(back_out.at[:, : EXPERTS - 1], send_sem.at[5])
+        sent(peer_out.at[:, : group_size - 1], sum_send)
+    sent(back_out.at[:, : EXPERTS - 1], back_send)
 
 
 def per_device(
@@ -531,8 +550,9 @@
     sources = lax.axis_size("ep")
     group_size = sources // EXPERTS
     half = model_width // 2
-    piece = half // PIECES
-    chunk = half // CHUNKS
+    pieces = parts_of(half, PIECE_SHARES)
+    strips = half // STRIP
+    chunks = parts_of(half, CHUNK_SHARES)
     hidden_units = w_down.shape[0]
     total_rows = sources * CAP
     peers = max(group_size - 1, 1)
@@ -561,6 +581,10 @@
         w_down,
     )
     staged = operands[:9] + operands[11:14]
+
+    def each(parts, shape, dtype=narrow):
+        return tuple(pltpu.VMEM((*shape, size), dtype) for _, size in parts)
+
     new_tokens, new_carried = pl.pallas_call(
         functools.partial(layer_kernel, group_size),
         out_shape=(
@@ -582,30 +606,35 @@
             pltpu.VMEM((OUT_PARTS, count_rows, model_width // OUT_PARTS), narrow),
             pltpu.VMEM((count_rows, model_width), narrow),
             pltpu.VMEM((count_rows, model_width), narrow),
-            pltpu.VMEM((CHUNKS, EXPERTS, CAP, chunk), narrow),
-            pltpu.VMEM((CHUNKS, 2, group_size, EXPERTS, CAP, chunk), narrow),
+            each(chunks, (EXPERTS, CAP)),
+            each(chunks, (2, group_size, EXPERTS, CAP)),
             pltpu.VMEM((hidden_units, total_rows), wide),
             pltpu.VMEM((hidden_units, total_rows), wide),
             pltpu.VMEM((hidden_units, total_rows), narrow),
             pltpu.VMEM((total_rows, hidden_units), narrow),
-            pltpu.VMEM((PIECES, total_rows, piece), narrow),
-            pltpu.VMEM((PIECES, total_rows, piece), narrow),
-            pltpu.VMEM((PIECES, group_size, EXPERTS, CAP, piece), wide),
-            pltpu.VMEM((PIECES, group_size, EXPERTS, CAP, piece), narrow),
-            pltpu.VMEM((PIECES, peers, EXPERTS, CAP, piece), narrow),
-            pltpu.VMEM((PIECES, EXPERTS, CAP, piece), narrow),
-            pltpu.VMEM((PIECES, EXPERTS, CAP, piece), narrow),
+            each(pieces, (total_rows,)),
+            each(pieces, (total_rows,)),
+            pltpu.VMEM((strips, group_size, EXPERTS, CAP, STRIP), wide),
+            pltpu.VMEM((strips, group_size, EXPERTS, CAP, STRIP), narrow),
+            pltpu.VMEM((strips, peers, EXPERTS, CAP, STRIP), narrow),
+            pltpu.VMEM((strips, EXPERTS, CAP, STRIP), narrow),
+            pltpu.VMEM((strips, EXPERTS, CAP, STRIP), narrow),
             dma((len(staged) + model_width // width + OUT_PARTS,)),
             dma((2,)),
             dma,
             dma((OUT_PARTS,)),
-            dma((CHUNKS, EXPERTS)),
-            dma((CHUNKS, group_size)),
-            dma((CHUNKS,)),
-            dma((PIECES,)),
-            dma((PIECES,)),
-            dma((PIECES,)),
-            dma((6,)),
+            dma((len(chunks),)),
+            dma((len(chunks), EXPERTS)),
+            dma((len(chunks),)),
+            dma((len(chunks), group_size)),
+            dma((len(chunks),)),
+            dma((len(chunks),)),
+            dma((len(pieces),)),
+            dma((len(pieces),)),
+            dma,
+            dma((strips,)),
+            dma,
+            dma((strips,)),
         ],
         compiler_params=pltpu.CompilerParams(
             collective_id=0, has_side_effects=True, vmem_limit_bytes=50 * 1024 * 1024

time: 54.5 us -> 49.6 us (0.910)
  Pallas kernels: 52.2 us -> 47.3 us
    pallas_call x1, Pallas kernels: 52.2 us -> 47.3 us  [per_device(): pl.pallas_call(functools.partial(layer_kernel, group_size), out_shape=(ja...]
where the time goes in v2:
time: 49.6 us; the launch traced here: 49.4 us
  Pallas kernels  47.3 us (95%)
  local copies, waits for them, and re-layouts  1.52 us (3%)
  between operations  0.65 us (1%)
    pallas_call x1, Pallas kernels, per_device(): pl.pallas_call(functools.partial(layer_kernel, group_size), out_shape=(ja...  47.3 us
    unnamed x2, local copies, waits for them, and re-layouts  1.52 us

profile of v2, /device:TPU:0, one launch (start us, length us, event | category | flops | bytes accessed | tf_op | source)
XLA Modules:
  0.0 49.4 jit_solution(11213985134075788168)
XLA Ops:
  0.6 47.3 %shard_map.176 = (bf16[32,1536]{1,0:T(8,128)(2,1)S(1)}, f32[1536,128]{1,0:T(8,128)S(1)}) custom-call(bf16[32,3072]{1,0:T(8,128)(2,1)} %tokens_hbm.1, f32[1536,128]{1,0:T(8,128)} %bitcast.16, f32[48,64]{1,0:T(8,128)} %decay_hbm.1, f32[48,64]{1,0:T(8,128)} %frequency_hbm.1, f32[1,48]{1,0:T(1,128)} %bitcast.23, bf16[768,128]{1,0:T(8,128)(2,1)} %bitcast.17, ...), custom_call_target="tpu_custom_call" | custom-call | tf_op jit(solution)/shard_map/pallas_call | solution.py:588
  47.9 0.6 %copy.21 = bf16[32,1536]{1,0:T(8,128)(2,1)} copy(bf16[32,1536]{1,0:T(8,128)(2,1)S(1)} %get-tuple-element.8) | data formatting | bytes 196608
  48.6 0.9 %copy.22 = f32[32,48,128]{2,1,0:T(8,128)} copy(f32[32,48,128]{2,1,0:T(8,128)S(1)} %bitcast.13) | data formatting | bytes 1572864

commit v3 on v2

--- a/solution.py
+++ b/solution.py
@@ -21,7 +21,7 @@
 UNIT_PARTS = 2
 LANES = 128
 LATE_PART = 1
-OUT_PARTS = 4
+OUT_PARTS = 2
 WEIGHT_PARTS = 3
 
 
@@ -386,26 +386,17 @@
 
     height = hidden_units // UNIT_PARTS
 
-    def accumulate(index, number):
+    def accumulate(index, side, number, stage):
         begin, size = chunks[index]
         units = slice(number * height, (number + 1) * height)
-        arrived = rows_buf[index]
-
-        def project(weights):
-            value = dot_transposed(
-                weights[units, begin : begin + size], arrived[0].reshape(total_rows, size)
-            )
-            return value + dot_transposed(
-                weights[units, half + begin : half + begin + size],
-                arrived[1].reshape(total_rows, size),
-            )
-
-        gated = project(gate)
-        upward = project(up)
-        if index:
+        columns = pl.ds(pl.multiple_of(side * half + begin, LANES), size)
+        arrived = rows_buf[index][side].reshape(total_rows, size)
+        gated = dot_transposed(gate[units, columns], arrived)
+        upward = dot_transposed(up[units, columns], arrived)
+        if stage:
             gated = gate_sum[units, :] + gated
             upward = up_sum[units, :] + upward
-        if index < len(chunks) - 1:
+        if stage < 2 * len(chunks) - 1:
             gate_sum[units, :] = gated
             up_sum[units, :] = upward
         else:
@@ -423,9 +414,11 @@
         if index == 0:
             cross(0)
             pltpu.make_async_copy(gate_up, gate_up, weight_sem.at[0]).wait()
+        for number in range(UNIT_PARTS):
+            accumulate(index, core, number, 2 * index)
         from_core(index).wait_recv()
         for number in range(UNIT_PARTS):
-            accumulate(index, number)
+            accumulate(index, other, number, 2 * index + 1)
             if number == 0 and index + 1 < len(chunks):
                 cross(index + 1)
     transpose(0, hidden_units)

time: 49.6 us -> 48.6 us (0.980)
  Pallas kernels: 47.3 us -> 46.3 us
    pallas_call x1, Pallas kernels: 47.3 us -> 46.3 us  [per_device(): pl.pallas_call(functools.partial(layer_kernel, group_size), out_shape=(ja...]
where the time goes in v3:
time: 48.6 us; the launch traced here: 48.4 us
  Pallas kernels  46.3 us (95%)
  local copies, waits for them, and re-layouts  1.52 us (3%)
  between operations  0.65 us (1%)
    pallas_call x1, Pallas kernels, per_device(): pl.pallas_call(functools.partial(layer_kernel, group_size), out_shape=(ja...  46.3 us
    unnamed x2, local copies, waits for them, and re-layouts  1.52 us

profile of v3, /device:TPU:0, one launch (start us, length us, event | category | flops | bytes accessed | tf_op | source)
XLA Modules:
  0.0 48.4 jit_solution(12425060100868965216)
XLA Ops:
  0.6 46.3 %shard_map.176 = (bf16[32,1536]{1,0:T(8,128)(2,1)S(1)}, f32[1536,128]{1,0:T(8,128)S(1)}) custom-call(bf16[32,3072]{1,0:T(8,128)(2,1)} %tokens_hbm.1, f32[1536,128]{1,0:T(8,128)} %bitcast.16, f32[48,64]{1,0:T(8,128)} %decay_hbm.1, f32[48,64]{1,0:T(8,128)} %frequency_hbm.1, f32[1,48]{1,0:T(1,128)} %bitcast.23, bf16[768,128]{1,0:T(8,128)(2,1)} %bitcast.17, ...), custom_call_target="tpu_custom_call" | custom-call | tf_op jit(solution)/shard_map/pallas_call | solution.py:581
  46.9 0.6 %copy.21 = bf16[32,1536]{1,0:T(8,128)(2,1)} copy(bf16[32,1536]{1,0:T(8,128)(2,1)S(1)} %get-tuple-element.8) | data formatting | bytes 196608
  47.5 0.9 %copy.22 = f32[32,48,128]{2,1,0:T(8,128)} copy(f32[32,48,128]{2,1,0:T(8,128)S(1)} %bitcast.13) | data formatting | bytes 1572864

commit v4 on v3

--- a/solution.py
+++ b/solution.py
@@ -18,7 +18,7 @@
 CHUNK_SHARES = (3, 3)
 PIECE_SHARES = (2, 2, 2)
 STRIP = 256
-UNIT_PARTS = 2
+UNIT_PARTS = 1
 LANES = 128
 LATE_PART = 1
 OUT_PARTS = 2

time: 48.6 us -> 48.4 us (level)
  no operation moved by 1% of the time
where the time goes in v4:
time: 48.4 us; the launch traced here: 48.2 us
  Pallas kernels  46.1 us (95%)
  local copies, waits for them, and re-layouts  1.52 us (3%)
  between operations  0.65 us (1%)
    pallas_call x1, Pallas kernels, per_device(): pl.pallas_call(functools.partial(layer_kernel, group_size), out_shape=(ja...  46.1 us
    unnamed x2, local copies, waits for them, and re-layouts  1.52 us

profile of v4, /device:TPU:0, one launch (start us, length us, event | category | flops | bytes accessed | tf_op | source)
XLA Modules:
  0.0 48.2 jit_solution(12787574469463299271)
XLA Ops:
  0.6 46.1 %shard_map.176 = (bf16[32,1536]{1,0:T(8,128)(2,1)S(1)}, f32[1536,128]{1,0:T(8,128)S(1)}) custom-call(bf16[32,3072]{1,0:T(8,128)(2,1)} %tokens_hbm.1, f32[1536,128]{1,0:T(8,128)} %bitcast.16, f32[48,64]{1,0:T(8,128)} %decay_hbm.1, f32[48,64]{1,0:T(8,128)} %frequency_hbm.1, f32[1,48]{1,0:T(1,128)} %bitcast.23, bf16[768,128]{1,0:T(8,128)(2,1)} %bitcast.17, ...), custom_call_target="tpu_custom_call" | custom-call | tf_op jit(solution)/shard_map/pallas_call | solution.py:581
  46.7 0.6 %copy.21 = bf16[32,1536]{1,0:T(8,128)(2,1)} copy(bf16[32,1536]{1,0:T(8,128)(2,1)S(1)} %get-tuple-element.8) | data formatting | bytes 196608
  47.4 0.9 %copy.22 = f32[32,48,128]{2,1,0:T(8,128)} copy(f32[32,48,128]{2,1,0:T(8,128)S(1)} %bitcast.13) | data formatting | bytes 1572864
